TPU v7x, 32 devices: a whole 2x2x4 slice. The times are simulated.
32 devices in a mesh: sp: 8 (over z, y), tp: 4 (over x, core).
Axes of the slice: x: 2, y: 2, z: 4, core: 2. Of those that a mesh axis runs over, the one named last changes fastest.
Arguments:
- latents: bfloat16 [2560, 2048], P(('sp', 'tp')), may hold values from -12.5 to 12.5, as said below
- context: bfloat16 [1024, 2048], P('sp'), may hold values from -120 to 120, as said below
- cond_vec: float32 [2048], replicated, may hold values from -6 to 6
- ctx_vec: float32 [2048], replicated, may hold values from -6 to 6
- shift_w: bfloat16 [2048, 2048], P('sp', 'tp'), may hold values from -0.125 to 0.125
- scale_w: bfloat16 [2048, 2048], P('sp', 'tp'), may hold values from -0.125 to 0.125
- modgate_w: bfloat16 [2048, 2048], P('sp', 'tp'), may hold values from -0.125 to 0.125
- query_down_weight: bfloat16 [2048, 512], replicated, may hold values from -0.125 to 0.125
- latent_down_weight: bfloat16 [2048, 256], replicated, may hold values from -0.125 to 0.125
- rot_down: bfloat16 [2048, 32], replicated, may hold values from -0.125 to 0.125
- gate_w: bfloat16 [2048, 2048], P(None, 'tp'), may hold values from -0.125 to 0.125
- query_norm_gain: float32 [512], replicated, may hold values from 0.1 to 1.9
- latent_norm_gain: float32 [256], replicated, may hold values from 0.1 to 1.9
- query_plain_weight: bfloat16 [512, 2048], P(None, 'tp'), may hold values from -0.25 to 0.25
- query_rotary_weight: bfloat16 [512, 1024], P(None, 'tp'), may hold values from -0.25 to 0.25
- key_expand_weight: bfloat16 [256, 2048], P(None, 'tp'), may hold values from -0.375 to 0.375
- value_expand_weight: bfloat16 [256, 2048], P(None, 'tp'), may hold values from -0.375 to 0.375
- out_w: bfloat16 [2048, 2048], P('tp'), may hold values from -0.5 to 0.5
- norm_gain: float32 [2048], replicated, may hold values from 0.1 to 1.9
- norm_bias: float32 [2048], replicated, may hold values from -3 to 3
Outputs:
- mixed_out: bfloat16 [2560, 2048], P(('sp', 'tp'))
Inputs may be any that keep to these rules, and one draw needn't show every extreme that they name: `latents`: latent rows are noise plus three slow waves along the whole sequence. Most context rows have their own scales of 1 to 3; a few rows may be far larger.
All inputs are finite; a program needn't handle non-finite values.
Results may differ from a plain program's by a relative error of at most 0.024.
The roundings to bfloat16 on the way count: a program that leaves them out, or rounds other values in their place, can miss the bound.
Values may be sent and summed in bfloat16 or wider, within the bound.
No kernel may reach another device: no remote copies, remote signals or barrier semaphores. Data moves between devices by JAX's collectives and lax.ppermute only.
A program may use at most 128 MiB of HBM per device.

v0:
```python
import jax
import jax.numpy as jnp
from jax import lax
from jax.sharding import PartitionSpec as P

PLAIN_HEAD_SIZE = 64
ROTARY_SIZE = 32
VALUE_HEAD_SIZE = 64
GRID_W = 64
rope_base = 10000.0
norm_floor = 1e-06
residual_weight = 2.0**0.5
score_floor = -1e30


def rms_scale(values, gain):
    return values * lax.rsqrt(jnp.mean(values * values, axis=-1, keepdims=True) + norm_floor) * gain


def rotate(values, positions):
    pair_count = ROTARY_SIZE // 4
    inverse = rope_base ** (-jnp.arange(pair_count, dtype=jnp.float32) / pair_count)
    grid_row = (positions // GRID_W).astype(jnp.float32)
    grid_col = (positions % GRID_W).astype(jnp.float32)
    angles = jnp.stack([grid_row[:, None] * inverse, grid_col[:, None] * inverse], axis=1)
    cosine = jnp.cos(angles)[:, None, :, None, :]
    sine_part = jnp.sin(angles)[:, None, :, None, :]
    shaped = values.reshape(values.shape[0], -1, 2, 2, pair_count)
    first_part = shaped[:, :, :, 0:1, :]
    second = shaped[:, :, :, 1:2, :]
    turned = jnp.concatenate(
        [first_part * cosine - second * sine_part, second * cosine + first_part * sine_part], axis=3
    )
    return turned.reshape(values.shape)


def project(rows, weight):
    return jnp.dot(rows, weight, preferred_element_type=jnp.float32)


def per_device(
    latents,
    context,
    cond_vec,
    ctx_vec,
    shift_w,
    scale_w,
    modgate_w,
    query_down_weight,
    latent_down_weight,
    rot_down,
    gate_w,
    query_norm_gain,
    latent_norm_gain,
    query_plain_weight,
    query_rotary_weight,
    key_expand_weight,
    value_expand_weight,
    out_w,
    norm_gain,
    norm_bias,
):
    width_tp = lax.axis_size("tp")
    block_rows = latents.shape[0]
    seq_rows = block_rows * width_tp
    slab_rows = shift_w.shape[0]
    sp_index = lax.axis_index("sp")
    cond_rows = jnp.stack([jax.nn.silu(cond_vec), jax.nn.silu(ctx_vec)]).astype(jnp.bfloat16)
    cond_here = lax.dynamic_slice_in_dim(cond_rows, sp_index * slab_rows, slab_rows, 1)
    shift_part = project(cond_here, shift_w)
    scale_part = project(cond_here, scale_w)
    gate_part = project(cond_here, modgate_w)
    columns = shift_w.shape[1]
    corner = (jnp.int32(0), lax.axis_index("tp") * columns)
    blank_rows = jnp.zeros((2, latents.shape[1]), jnp.float32)
    shift_vec, scale_vec, gate_vec = lax.psum(
        (
            lax.dynamic_update_slice(blank_rows, shift_part, corner),
            lax.dynamic_update_slice(blank_rows, scale_part, corner),
            lax.dynamic_update_slice(blank_rows, gate_part, corner),
        ),
        ("sp", "tp"),
    )
    latent_in = (latents.astype(jnp.float32) * (1.0 + scale_vec[0]) + shift_vec[0]).astype(
        jnp.bfloat16
    )
    context_in = (context.astype(jnp.float32) * (1.0 + scale_vec[1]) + shift_vec[1]).astype(
        jnp.bfloat16
    )
    heads_here = gate_w.shape[1] // VALUE_HEAD_SIZE
    rows_part = lax.all_gather(latent_in, "tp", axis=0, tiled=True)
    positions = sp_index * seq_rows + jnp.arange(rows_part.shape[0], dtype=jnp.int32)
    q_codes = rms_scale(project(rows_part, query_down_weight), query_norm_gain).astype(jnp.bfloat16)
    kv_codes = rms_scale(project(rows_part, latent_down_weight), latent_norm_gain).astype(
        jnp.bfloat16
    )
    key_rot = rotate(project(rows_part, rot_down), positions).astype(jnp.bfloat16)
    gate_act = project(rows_part, gate_w).astype(jnp.bfloat16)
    project_q_cont = project(q_codes, query_plain_weight).astype(jnp.bfloat16)
    project_q_rot = rotate(project(q_codes, query_rotary_weight), positions).astype(jnp.bfloat16)
    joined = jnp.concatenate([project_q_cont, project_q_rot, gate_act, kv_codes, key_rot], axis=1)
    edge_one = query_plain_weight.shape[1]
    edge_two = edge_one + query_rotary_weight.shape[1]
    edge_three = edge_two + gate_w.shape[1]
    edge_four = edge_three + latent_down_weight.shape[1]
    q_cont = joined[:, :edge_one].reshape(seq_rows, heads_here, PLAIN_HEAD_SIZE)
    q_rot = joined[:, edge_one:edge_two].reshape(seq_rows, heads_here, ROTARY_SIZE)
    gate_act = joined[:, edge_two:edge_three]
    kv_codes = joined[:, edge_three:edge_four]
    key_rot = joined[:, edge_four:]
    ctx_codes = rms_scale(project(context_in, latent_down_weight), latent_norm_gain).astype(
        jnp.bfloat16
    )
    ctx_rot = project(context_in, rot_down).astype(jnp.bfloat16)
    score_scale = (PLAIN_HEAD_SIZE + ROTARY_SIZE) ** (-0.5)

    def expand(codes):
        return (
            project(codes, key_expand_weight).astype(jnp.bfloat16),
            project(codes, value_expand_weight).astype(jnp.bfloat16),
        )

    def attend(running, key_block, value_block, rotary):
        row_top, row_total, weighted = running
        key_count = key_block.shape[0]
        scores = jnp.einsum(
            "qhd,khd->hqk",
            q_cont,
            key_block.reshape(key_count, heads_here, PLAIN_HEAD_SIZE),
            preferred_element_type=jnp.float32,
        )
        scores = (
            scores + jnp.einsum("qhd,kd->hqk", q_rot, rotary, preferred_element_type=jnp.float32)
        ) * score_scale
        new_top = jnp.maximum(row_top, jnp.max(scores, axis=-1))
        weights = jnp.exp(scores - new_top[:, :, None])
        factor = jnp.exp(row_top - new_top)
        row_total = row_total * factor + jnp.sum(weights, axis=-1)
        weighted = weighted * factor[:, :, None] + jnp.einsum(
            "hqk,khd->hqd",
            weights.astype(jnp.bfloat16),
            value_block.reshape(key_count, heads_here, VALUE_HEAD_SIZE),
            preferred_element_type=jnp.float32,
        )
        return (new_top, row_total, weighted)

    start_state = (
        jnp.full((heads_here, seq_rows), score_floor, jnp.float32),
        jnp.zeros((heads_here, seq_rows), jnp.float32),
        jnp.zeros((heads_here, seq_rows, VALUE_HEAD_SIZE), jnp.float32),
    )
    ctx_all_codes, ctx_all_rot = (
        lax.all_gather(ctx_codes, "sp", axis=0, tiled=True),
        lax.all_gather(ctx_rot, "sp", axis=0, tiled=True),
    )
    ctx_keys, ctx_values = expand(ctx_all_codes)
    running = attend(start_state, ctx_keys, ctx_values, ctx_all_rot)
    pieces = (
        lax.all_gather(kv_codes, "sp", axis=0, tiled=True),
        lax.all_gather(key_rot, "sp", axis=0, tiled=True),
    )
    total_rows = pieces[0].shape[0]
    unit_count = total_rows // seq_rows
    grouped = max(
        [1]
        + [
            divisor
            for divisor in range(1, unit_count + 1)
            if unit_count % divisor == 0 and divisor * seq_rows <= 1024
        ]
    )
    blocked = tuple(
        (
            member.reshape(unit_count // grouped, grouped * seq_rows, member.shape[1])
            for member in pieces
        )
    )

    def one_block(carried, members):
        key_block, value_block = expand(members[0])
        return (attend(carried, key_block, value_block, members[1]), None)

    result, unused = lax.scan(one_block, running, blocked)
    running = result
    row_top, row_total, weighted = running
    attended = jnp.transpose(weighted / row_total[:, :, None], (1, 0, 2)).reshape(
        seq_rows, heads_here * VALUE_HEAD_SIZE
    )
    gated = (attended * jax.nn.silu(gate_act.astype(jnp.float32))).astype(jnp.bfloat16)
    branch = lax.psum_scatter(
        project(gated, out_w).astype(jnp.bfloat16), "tp", scatter_dimension=0, tiled=True
    ).astype(jnp.float32)
    blended = residual_weight * latents.astype(jnp.float32) + gate_vec[0] * branch
    row_mean = jnp.mean(blended, axis=-1, keepdims=True)
    centred = blended - row_mean
    row_var = jnp.mean(centred * centred, axis=-1, keepdims=True)
    return (centred * lax.rsqrt(row_var + norm_floor) * norm_gain + norm_bias).astype(jnp.bfloat16)


def solution(mesh):
    in_specs = (
        P(("sp", "tp"), None),
        P("sp", None),
        P(),
        P(),
        P("sp", "tp"),
        P("sp", "tp"),
        P("sp", "tp"),
        P(),
        P(),
        P(),
        P(None, "tp"),
        P(),
        P(),
        P(None, "tp"),
        P(None, "tp"),
        P(None, "tp"),
        P(None, "tp"),
        P("tp", None),
        P(),
        P(),
    )
    out_specs = P(("sp", "tp"), None)
    return jax.shard_map(
        per_device, mesh=mesh, in_specs=in_specs, out_specs=out_specs, check_vma=False
    )
```

profile of v0, /device:TPU:0, one launch (start us, length us, event | category | flops | bytes accessed | tf_op | source)
XLA Modules:
  0.0 249.4 jit_solution(9773118889546091030)
XLA Ops:
  11.7 42.5 %all-reduce = (f32[2,2048]{1,0:T(2,128)S(1)}, f32[2,2048]{1,0:T(2,128)S(1)}, f32[2,2048]{1,0:T(2,128)S(1)}) all-reduce(f32[2,2048]{1,0:T(2,128)S(1)} %convolution_dynamic-update-slice_fusion, f32[2,2048]{1,0:T(2,128)S(1)} %convolution_dynamic-update-slice_fusion.1, ...), channel_id=1, replica_groups=mesh['sp'=8,'tp'=4] {'sp','tp'}, use_global_device_ids=true, to_apply=%region_2.3 | all-reduce | flops 12288 | bytes 98304 | tf_op jit(solution)/shard_map/psum | solution.py:76
  54.2 1.8 fusion.30
  57.4 26.1 %all_gather.17 = bf16[1024,32]{0,1:T(8,128)(2,1)S(1)} all-gather(bf16[128,32]{0,1:T(8,128)(2,1)S(1)} %convolution_convert_fusion.7), channel_id=1, replica_groups=mesh['sp'=8,'tp'=4] {'sp'}, dimensions={0}, use_global_device_ids=true | all-gather | bytes 73728 | tf_op jit(solution)/shard_map/all_gather | solution.py:154
  83.7 1.6 multiply_reduce_fusion.3
  85.4 31.5 %all_gather.16 = bf16[1024,256]{1,0:T(8,128)(2,1)S(1)} all-gather(bf16[128,256]{1,0:T(8,128)(2,1)S(1)} %multiply_convert_fusion.3), channel_id=1, replica_groups=mesh['sp'=8,'tp'=4] {'sp'}, dimensions={0}, use_global_device_ids=true | all-gather | bytes 589824 | tf_op jit(solution)/shard_map/all_gather | solution.py:153
  116.9 1.5 convolution_convert_fusion.4
  119.9 3.0 %multiply_reduce_fusion.1 = (f32[320]{0:T(512)S(1)}, f32[320,512]{1,0:T(8,128)S(1)}) fusion(bf16[320,2048]{1,0:T(8,128)(2,1)} %all-gather.4.cloned.1.call-done, bf16[2048,512]{1,0:T(8,128)(2,1)} %param.29), kind=kOutput, calls=%fused_computation.49 | convolution fusion | flops 671416000 | bytes 4064512 | tf_op jit(solution)/shard_map/dot_general | solution.py:38
  123.9 2.2 multiply_reduce_fusion.2
  127.0 1.8 fusion.58
  129.0 31.2 %all-gather = bf16[8,320,32]{1,2,0:T(8,128)(2,1)S(1)} all-gather(bf16[1,320,32]{1,2,0:T(8,128)(2,1)S(1)} %bitcast.115), channel_id=1, replica_groups=mesh['sp'=8,'tp'=4] {'sp'}, dimensions={0}, use_global_device_ids=true | all-gather | bytes 184320 | tf_op jit(solution)/shard_map/all_gather | solution.py:160
  161.2 1.6 fusion.34
  162.8 1.8 fusion.56
  164.6 2.1 fusion.20
  166.7 2.2 fusion.24
  169.0 37.6 %while.14 = (s32[]{:T(128)}, f32[8,320]{1,0:T(8,128)S(1)}, f32[8,320]{1,0:T(8,128)S(1)}, f32[8,320,64]{1,2,0:T(8,128)S(1)}, bf16[4,640,256]{2,1,0:T(8,128)(2,1)}...) while((s32[]{:T(128)}, f32[8,320]{1,0:T(8,128)S(1)}, ...), condition=%wide.region_11.12_spmd, body=%wide.region_8.11_spmd.sunk | while | flops 872289280 | bytes 39624860 | solution.py:183
  169.0 1.5 convolution_convert_fusion.10
  171.6 2.2 fusion.112
  173.7 1.5 fusion.113
  176.7 1.7 fusion.114
  178.4 1.5 convolution_convert_fusion.10
  181.0 2.2 fusion.112
  183.1 1.5 fusion.113
  186.1 1.7 fusion.114
  190.3 2.2 fusion.112
  192.5 1.5 fusion.113
  195.5 1.7 fusion.114
  199.7 2.2 fusion.112
  201.9 1.5 fusion.113
  204.9 1.7 fusion.114
  209.0 4.8 %convolution_convert_fusion.2 = bf16[320,2048]{1,0:T(8,128)(2,1)} fusion(bf16[512,2048]{1,0:T(8,128)(2,1)S(1)} %copy-done, f32[320,512]{1,0:T(8,128)S(1)} %copy.40, bf16[320,2048]{1,0:T(8,128)(2,1)} %all-gather.4.cloned.1.call-done, bf16[2048,512]{1,0:T(8,128)(2,1)} %param.32), kind=kOutput, calls=%fused_computation.28 | convolution fusion | flops 1344143360 | bytes 7471104 | tf_op jit(solution)/shard_map/dot_general | solution.py:38
  213.8 24.7 %reduce-scatter.2.cloned.1.call-done = bf16[80,2048]{1,0:T(8,128)(2,1)} async-done(((bf16[320,2048]{1,0:T(8,128)(2,1)}), bf16[80,2048]{1,0:T(8,128)(2,1)}) %reduce-scatter.2.cloned.1.call-update) | async-done | bytes 327696 | tf_op jit(solution)/shard_map/reduce_scatter | solution.py:190
  241.0 1.9 add_convert_fusion.1
  (107 shorter events, 29.1 us)
Async XLA Ops:
  6.5 202.4 %copy-start = (bf16[512,2048]{1,0:T(8,128)(2,1)S(1)}, bf16[512,2048]{1,0:T(8,128)(2,1)}, u32[]{:S(2)}) copy-start(bf16[512,2048]{1,0:T(8,128)(2,1)} %param.39) | copy-start | bytes 6291460
  6.5 77.2 %copy-start.14 = (bf16[128,2048]{1,0:T(8,128)(2,1)S(1)}, bf16[128,2048]{1,0:T(8,128)(2,1)}, u32[]{:S(2)}) copy-start(bf16[128,2048]{1,0:T(8,128)(2,1)} %param.23) | copy-start | bytes 1572868
  6.5 78.8 %copy-start.13 = (f32[256]{0:T(256)S(1)}, f32[256]{0:T(256)}, u32[]{:S(2)}) copy-start(f32[256]{0:T(256)} %param.34) | copy-start | bytes 3076
  6.5 113.3 %all-gather.4.cloned.1.call-start = ((), (), s32[]{:S(2)}) async-start(), calls=%async_computation.1 | async-start | bytes 1638400 | tf_op jit(solution)/shard_map/all_gather | solution.py:91
  10.5 106.4 %copy-start.1 = (bf16[256,512]{1,0:T(8,128)(2,1)S(1)}, bf16[256,512]{1,0:T(8,128)(2,1)}, u32[]{:S(2)}) copy-start(bf16[256,512]{1,0:T(8,128)(2,1)} %param.37) | copy-start | bytes 786436
  56.0 113.0 %all-gather.6.cloned.1.call-start = ((), (), s32[]{:S(2)}) async-start(), calls=%async_computation.2 | async-start | bytes 1474560 | tf_op jit(solution)/shard_map/all_gather | solution.py:159
  56.1 62.3 %copy-start.2 = (bf16[256,512]{1,0:T(8,128)(2,1)S(1)}, bf16[256,512]{1,0:T(8,128)(2,1)}, u32[]{:S(2)}) copy-start(bf16[256,512]{1,0:T(8,128)(2,1)} %param.38) | copy-start | bytes 786436
  119.9 3.0 %copy-start.8 = (bf16[512,256]{1,0:T(8,128)(2,1)S(1)}, bf16[512,256]{1,0:T(8,128)(2,1)}, u32[]{:S(2)}) copy-start(bf16[512,256]{1,0:T(8,128)(2,1)} %param.36) | copy-start | bytes 786436
  119.9 3.0 %copy-start.12 = (f32[512]{0:T(512)S(1)}, f32[512]{0:T(512)}, u32[]{:S(2)}) copy-start(f32[512]{0:T(512)} %param.33) | copy-start | bytes 6148
  119.9 3.4 %copy-start.7 = (bf16[512,512]{1,0:T(8,128)(2,1)S(1)}, bf16[512,512]{1,0:T(8,128)(2,1)}, u32[]{:S(2)}) copy-start(bf16[512,512]{1,0:T(8,128)(2,1)} %param.35) | copy-start | bytes 1572868
  123.7 3.3 %copy-start.9 = (bf16[2048,32]{0,1:T(8,128)(2,1)S(1)}, bf16[2048,32]{0,1:T(8,128)(2,1)}, u32[]{:S(2)}) copy-start(bf16[2048,32]{0,1:T(8,128)(2,1)} %param.31) | copy-start | bytes 393220
  127.0 111.5 %reduce-scatter.2.cloned.1.call-start = ((), (), s32[]{:S(2)}) async-start(), calls=%async_computation.3 | async-start | bytes 1638400 | tf_op jit(solution)/shard_map/reduce_scatter | solution.py:190
  161.2 1.6 copy-start.5
  164.6 2.2 copy-start.6
  173.7 1.6 copy-start.3
  183.1 1.6 copy-start.3
  192.5 1.6 copy-start.3
  201.9 1.6 copy-start.3
  209.0 29.5 %copy-start.4 = (bf16[80,2048]{1,0:T(8,128)(2,1)S(1)}, bf16[80,2048]{1,0:T(8,128)(2,1)}, u32[]{:S(2)}) copy-start(bf16[80,2048]{1,0:T(8,128)(2,1)} %param.22) | copy-start | bytes 983044
  213.8 27.2 %copy-start.10 = (f32[2048]{0:T(1024)S(1)}, f32[2048]{0:T(1024)}, u32[]{:S(2)}) copy-start(f32[2048]{0:T(1024)} %param.41) | copy-start | bytes 24580
  213.8 27.2 %copy-start.11 = (f32[2048]{0:T(1024)S(1)}, f32[2048]{0:T(1024)}, u32[]{:S(2)}) copy-start(f32[2048]{0:T(1024)} %param.40) | copy-start | bytes 24580
Sparse Core Ops, SparseCore 0:
  56.1 17.9 all-gather.3
  127.1 40.2 all-gather.5
  213.9 24.5 reduce-scatter.1
where the time goes:
time: 251 us; the launch traced here: 249 us
  blocking collectives  131 us (52%)
  matrix products  58.6 us (23%)
  waiting for transfers between devices  24.7 us (10%)
  other arithmetic  18.4 us (7%)
  between operations  13.5 us (5%)
  local copies, waits for them, and re-layouts  2.64 us (1%)
    psum x1, blocking collectives, per_device(): lax.psum((lax.dynamic_update_slice(blank_rows, shift_part, corner), lax.d...  42.5 us
    dot_general x21, matrix products, project(): return jnp.dot(rows, weight, preferred_element_type=jnp.float32)  33.4 us
    all_gather x1, blocking collectives, per_device(): lax.all_gather(ctx_codes, 'sp', axis=0, tiled=True)  31.5 us
    all_gather x1, blocking collectives, per_device(): lax.all_gather(key_rot, 'sp', axis=0, tiled=True)  31.2 us
    all_gather x1, blocking collectives, per_device(): lax.all_gather(ctx_rot, 'sp', axis=0, tiled=True)  26.1 us
    reduce_scatter x1, waiting for transfers between devices, per_device(): lax.psum_scatter(project(gated, out_w).astype(jnp.bfloat16), 'tp', scatte...  24.7 us
    dot_general x5, matrix products, attend(): jnp.einsum('qhd,kd->hqk', q_rot, rotary, preferred_element_type=jnp.float32)  10.2 us
    dot_general x5, matrix products, attend(): jnp.einsum('hqk,khd->hqd', weights.astype(jnp.bfloat16), value_block.resh...  8.97 us
  transfers between devices with their start and end apart: 3, of which 1 were waited for; matrix products, arithmetic and copies ran while one was open for 7% of the time, Pallas kernels for 0%

commit v1 on v0

--- a/solution.py
+++ b/solution.py
@@ -11,6 +11,13 @@
 norm_floor = 1e-06
 residual_weight = 2.0**0.5
 score_floor = -1e30
+
+
+def exchange_gather(array, axis, d):
+    n_dev = lax.axis_size(axis)
+    shards = jnp.stack([array for _ in range(n_dev)])
+    shards = lax.all_to_all(shards, axis, split_axis=0, concat_axis=0)
+    return jnp.concatenate(shards, axis=d)
 
 
 def rms_scale(values, gain):
@@ -151,7 +158,7 @@
     )
     ctx_all_codes, ctx_all_rot = (
         lax.all_gather(ctx_codes, "sp", axis=0, tiled=True),
-        lax.all_gather(ctx_rot, "sp", axis=0, tiled=True),
+        exchange_gather(ctx_rot, "sp", 0),
     )
     ctx_keys, ctx_values = expand(ctx_all_codes)
     running = attend(start_state, ctx_keys, ctx_values, ctx_all_rot)

time: 251 us -> 233 us (0.928)
  blocking collectives: 131 us -> 106 us
  starting transfers between devices: 0.09 us -> 5.44 us
    all_gather x1 -> x0, blocking collectives: 26.1 us -> none  [per_device(): lax.all_gather(ctx_rot, 'sp', axis=0, tiled=True)]
    all_to_all x0 -> x1, starting transfers between devices: none -> 5.32 us  [exchange_gather(): shards = lax.all_to_all(shards, axis, split_axis=0, concat_axis=0)]
  transfers between devices with their start and end apart: 3 -> 4, of which waited for: 1 -> 2; matrix products, arithmetic and copies ran while one was open for 7% -> 7% of each run, Pallas kernels for 0% -> 0%
where the time goes in v1:
time: 233 us; the launch traced here: 232 us
  blocking collectives  106 us (45%)
  matrix products  58.5 us (25%)
  waiting for transfers between devices  26.3 us (11%)
  other arithmetic  18.4 us (8%)
  between operations  13.5 us (6%)
  starting transfers between devices  5.44 us (2%)
  local copies, waits for them, and re-layouts  3.35 us (1%)
    psum x1, blocking collectives, per_device(): lax.psum((lax.dynamic_update_slice(blank_rows, shift_part, corner), lax.d...  42.4 us
    dot_general x21, matrix products, project(): return jnp.dot(rows, weight, preferred_element_type=jnp.float32)  33.4 us
    all_gather x1, blocking collectives, per_device(): lax.all_gather(ctx_codes, 'sp', axis=0, tiled=True)  32 us
    all_gather x1, blocking collectives, per_device(): lax.all_gather(key_rot, 'sp', axis=0, tiled=True)  31.4 us
    reduce_scatter x1, waiting for transfers between devices, per_device(): lax.psum_scatter(project(gated, out_w).astype(jnp.bfloat16), 'tp', scatte...  25.8 us
    dot_general x5, matrix products, attend(): jnp.einsum('qhd,kd->hqk', q_rot, rotary, preferred_element_type=jnp.float32)  10.2 us
    dot_general x5, matrix products, attend(): jnp.einsum('hqk,khd->hqd', weights.astype(jnp.bfloat16), value_block.resh...  8.97 us
    reduce_sum x5, other arithmetic, attend(): row_total = row_total * factor + jnp.sum(weights, axis=-1)  8.21 us
  transfers between devices with their start and end apart: 4, of which 2 were waited for; matrix products, arithmetic and copies ran while one was open for 7% of the time, Pallas kernels for 0%

profile of v1, /device:TPU:0, one launch (start us, length us, event | category | flops | bytes accessed | tf_op | source)
XLA Modules:
  0.0 231.7 jit_solution(16089523521966412484)
XLA Ops:
  11.7 42.4 %all-reduce = (f32[2,2048]{1,0:T(2,128)S(1)}, f32[2,2048]{1,0:T(2,128)S(1)}, f32[2,2048]{1,0:T(2,128)S(1)}) all-reduce(f32[2,2048]{1,0:T(2,128)S(1)} %convolution_dynamic-update-slice_fusion, f32[2,2048]{1,0:T(2,128)S(1)} %convolution_dynamic-update-slice_fusion.1, ...), channel_id=1, replica_groups=mesh['sp'=8,'tp'=4] {'sp','tp'}, use_global_device_ids=true, to_apply=%region_2.3 | all-reduce | flops 12288 | bytes 98304 | tf_op jit(solution)/shard_map/psum | solution.py:83
  56.1 5.3 %all-to-all-start = ((bf16[8,128,32]{1,2,0:T(8,128)(2,1)}), bf16[8,128,32]{1,2,0:T(8,128)(2,1)S(1)}, u32[]{:S(2)}, u32[]{:S(2)}) async-start(bf16[8,128,32]{1,2,0:T(8,128)(2,1)} %stack.40), calls=%async_computation | async-start | bytes 131072 | tf_op jit(solution)/shard_map/all_to_all | solution.py:19
  61.5 1.8 fusion.30
  63.4 1.6 multiply_reduce_fusion.3
  65.2 32.0 %all_gather.13 = bf16[1024,256]{1,0:T(8,128)(2,1)S(1)} all-gather(bf16[128,256]{1,0:T(8,128)(2,1)S(1)} %multiply_convert_fusion.3), channel_id=1, replica_groups=mesh['sp'=8,'tp'=4] {'sp'}, dimensions={0}, use_global_device_ids=true | all-gather | bytes 589824 | tf_op jit(solution)/shard_map/all_gather | solution.py:160
  98.7 1.5 convolution_convert_fusion.3
  100.5 3.0 %multiply_reduce_fusion.1 = (f32[320]{0:T(512)S(1)}, f32[320,512]{1,0:T(8,128)S(1)}) fusion(bf16[320,2048]{1,0:T(8,128)(2,1)} %all-gather.4.cloned.1.call-done, bf16[2048,512]{1,0:T(8,128)(2,1)} %param.29), kind=kOutput, calls=%fused_computation.49 | convolution fusion | flops 671416000 | bytes 4064512 | tf_op jit(solution)/shard_map/dot_general | solution.py:45
  104.5 2.2 multiply_reduce_fusion.2
  107.6 1.8 fusion.57
  109.6 31.4 %all-gather = bf16[8,320,32]{1,2,0:T(8,128)(2,1)S(1)} all-gather(bf16[1,320,32]{1,2,0:T(8,128)(2,1)S(1)} %bitcast.115), channel_id=1, replica_groups=mesh['sp'=8,'tp'=4] {'sp'}, dimensions={0}, use_global_device_ids=true | all-gather | bytes 184320 | tf_op jit(solution)/shard_map/all_gather | solution.py:167
  142.0 1.6 fusion.56
  143.6 1.7 fusion.54
  145.3 2.1 fusion.20
  147.5 2.2 fusion.24
  150.2 37.6 %while.14 = (s32[]{:T(128)}, f32[8,320]{1,0:T(8,128)S(1)}, f32[8,320]{1,0:T(8,128)S(1)}, f32[8,320,64]{1,2,0:T(8,128)S(1)}, bf16[4,640,256]{2,1,0:T(8,128)(2,1)}...) while((s32[]{:T(128)}, f32[8,320]{1,0:T(8,128)S(1)}, ...), condition=%wide.region_11.12_spmd, body=%wide.region_8.11_spmd.sunk | while | flops 872289280 | bytes 39624860 | solution.py:190
  152.7 2.2 fusion.112
  154.9 1.5 fusion.113
  157.8 1.7 fusion.114
  162.1 2.2 fusion.112
  164.3 1.5 fusion.113
  167.2 1.7 fusion.114
  168.9 1.5 convolution_convert_fusion.10
  171.5 2.2 fusion.112
  173.7 1.5 fusion.113
  176.6 1.7 fusion.114
  178.3 1.5 convolution_convert_fusion.10
  180.9 2.2 fusion.112
  183.1 1.5 fusion.113
  186.0 1.7 fusion.114
  190.1 4.8 %convolution_convert_fusion.2 = bf16[320,2048]{1,0:T(8,128)(2,1)} fusion(bf16[512,2048]{1,0:T(8,128)(2,1)S(1)} %copy-done, f32[320,512]{1,0:T(8,128)S(1)} %copy.41, bf16[320,2048]{1,0:T(8,128)(2,1)} %all-gather.4.cloned.1.call-done, bf16[2048,512]{1,0:T(8,128)(2,1)} %param.32), kind=kOutput, calls=%fused_computation.28 | convolution fusion | flops 1344143360 | bytes 7471104 | tf_op jit(solution)/shard_map/dot_general | solution.py:45
  194.9 25.8 %reduce-scatter.2.cloned.1.call-done = bf16[80,2048]{1,0:T(8,128)(2,1)} async-done(((bf16[320,2048]{1,0:T(8,128)(2,1)}), bf16[80,2048]{1,0:T(8,128)(2,1)}) %reduce-scatter.2.cloned.1.call-update) | async-done | bytes 327696 | tf_op jit(solution)/shard_map/reduce_scatter | solution.py:197
  223.2 1.9 add_convert_fusion.1
  (111 shorter events, 30.2 us)
Async XLA Ops:
  6.5 183.6 %copy-start = (bf16[512,2048]{1,0:T(8,128)(2,1)S(1)}, bf16[512,2048]{1,0:T(8,128)(2,1)}, u32[]{:S(2)}) copy-start(bf16[512,2048]{1,0:T(8,128)(2,1)} %param.39) | copy-start | bytes 6291460
  6.5 56.9 %copy-start.14 = (bf16[128,2048]{1,0:T(8,128)(2,1)S(1)}, bf16[128,2048]{1,0:T(8,128)(2,1)}, u32[]{:S(2)}) copy-start(bf16[128,2048]{1,0:T(8,128)(2,1)} %param.23) | copy-start | bytes 1572868
  6.5 58.5 %copy-start.13 = (f32[256]{0:T(256)S(1)}, f32[256]{0:T(256)}, u32[]{:S(2)}) copy-start(f32[256]{0:T(256)} %param.34) | copy-start | bytes 3076
  10.5 86.7 %copy-start.1 = (bf16[256,512]{1,0:T(8,128)(2,1)S(1)}, bf16[256,512]{1,0:T(8,128)(2,1)}, u32[]{:S(2)}) copy-start(bf16[256,512]{1,0:T(8,128)(2,1)} %param.37) | copy-start | bytes 786436
  56.1 44.2 %all-to-all-start = ((bf16[8,128,32]{1,2,0:T(8,128)(2,1)}), bf16[8,128,32]{1,2,0:T(8,128)(2,1)S(1)}, u32[]{:S(2)}, u32[]{:S(2)}) async-start(bf16[8,128,32]{1,2,0:T(8,128)(2,1)} %stack.40), calls=%async_computation | async-start | bytes 131072 | tf_op jit(solution)/shard_map/all_to_all | solution.py:19
  61.4 39.0 %all-gather.4.cloned.1.call-start = ((), (), s32[]{:S(2)}) async-start(), calls=%async_computation.2 | async-start | bytes 1638400 | tf_op jit(solution)/shard_map/all_gather | solution.py:98
  61.5 37.2 %copy-start.2 = (bf16[256,512]{1,0:T(8,128)(2,1)S(1)}, bf16[256,512]{1,0:T(8,128)(2,1)}, u32[]{:S(2)}) copy-start(bf16[256,512]{1,0:T(8,128)(2,1)} %param.38) | copy-start | bytes 786436
  63.3 86.8 %all-gather.6.cloned.1.call-start = ((), (), s32[]{:S(2)}) async-start(), calls=%async_computation.3 | async-start | bytes 1474560 | tf_op jit(solution)/shard_map/all_gather | solution.py:166
  100.4 3.1 %copy-start.8 = (bf16[512,256]{1,0:T(8,128)(2,1)S(1)}, bf16[512,256]{1,0:T(8,128)(2,1)}, u32[]{:S(2)}) copy-start(bf16[512,256]{1,0:T(8,128)(2,1)} %param.36) | copy-start | bytes 786436
  100.4 3.1 %copy-start.12 = (f32[512]{0:T(512)S(1)}, f32[512]{0:T(512)}, u32[]{:S(2)}) copy-start(f32[512]{0:T(512)} %param.33) | copy-start | bytes 6148
  100.5 3.4 %copy-start.7 = (bf16[512,512]{1,0:T(8,128)(2,1)S(1)}, bf16[512,512]{1,0:T(8,128)(2,1)}, u32[]{:S(2)}) copy-start(bf16[512,512]{1,0:T(8,128)(2,1)} %param.35) | copy-start | bytes 1572868
  104.3 3.3 %copy-start.9 = (bf16[2048,32]{0,1:T(8,128)(2,1)S(1)}, bf16[2048,32]{0,1:T(8,128)(2,1)}, u32[]{:S(2)}) copy-start(bf16[2048,32]{0,1:T(8,128)(2,1)} %param.31) | copy-start | bytes 393220
  107.6 113.2 %reduce-scatter.2.cloned.1.call-start = ((), (), s32[]{:S(2)}) async-start(), calls=%async_computation.4 | async-start | bytes 1638400 | tf_op jit(solution)/shard_map/reduce_scatter | solution.py:197
  142.0 1.6 copy-start.5
  145.3 2.2 copy-start.6
  154.9 1.6 copy-start.3
  164.3 1.6 copy-start.3
  173.7 1.6 copy-start.3
  183.1 1.6 copy-start.3
  190.1 30.6 %copy-start.4 = (bf16[80,2048]{1,0:T(8,128)(2,1)S(1)}, bf16[80,2048]{1,0:T(8,128)(2,1)}, u32[]{:S(2)}) copy-start(bf16[80,2048]{1,0:T(8,128)(2,1)} %param.22) | copy-start | bytes 983044
  194.9 28.3 %copy-start.10 = (f32[2048]{0:T(1024)S(1)}, f32[2048]{0:T(1024)}, u32[]{:S(2)}) copy-start(f32[2048]{0:T(1024)} %param.41) | copy-start | bytes 24580
  194.9 28.3 %copy-start.11 = (f32[2048]{0:T(1024)S(1)}, f32[2048]{0:T(1024)}, u32[]{:S(2)}) copy-start(f32[2048]{0:T(1024)} %param.40) | copy-start | bytes 24580
Sparse Core Ops, SparseCore 0:
  63.8 18.6 all-gather.3
  107.7 42.4 all-gather.5
  195.0 25.6 reduce-scatter.1
